TPU v7x, 32 devices: a whole 2x2x4 slice. The times are simulated.
32 devices in a mesh: grp: 2 (over x), ep: 16 (over z, y, core).
Axes of the slice: x: 2, y: 2, z: 4, core: 2. Of those that a mesh axis runs over, the one named last changes fastest.
Arguments:
- tokens: bfloat16 [128, 2048], P(('grp', 'ep')), parts along dimension 0, may hold values from -6 to 6
- prior_state: float32 [128, 32, 64, 64], P(('grp', 'ep')), parts along dimension 0, may hold values from -3 to 3
- receptance_matrix: bfloat16 [2048, 2048], P('ep'), may hold values from -0.125 to 0.125
- key_matrix: bfloat16 [2048, 2048], P('ep'), may hold values from -0.125 to 0.125
- value_matrix: bfloat16 [2048, 2048], P('ep'), may hold values from -0.125 to 0.125
- decay_lowrank_first: bfloat16 [2048, 64], replicated, may hold values from -0.125 to 0.125
- decay_lowrank_second: bfloat16 [64, 2048], replicated, may hold values from -1.5 to 1.5
- decay_channel_offset: float32 [2048], replicated, may hold values from -6 to 0
- correction_lowrank_first: bfloat16 [2048, 64], replicated, may hold values from -0.125 to 0.125
- correction_lowrank_second: bfloat16 [64, 2048], replicated, may hold values from -1.5 to 1.5
- correction_offset: float32 [2048], replicated, may hold values from -4 to 4
- gate_lowrank_first: bfloat16 [2048, 128], replicated, may hold values from -0.25 to 0.25
- gate_lowrank_second: bfloat16 [128, 2048], replicated, may hold values from -0.5 to 0.5
- key_rate_blend: float32 [2048], replicated, may hold values from 0.1 to 1.9
- self_token_scale: float32 [32, 64], replicated, may hold values from -1.2 to 1.2
- per_head_gain: float32 [2048], replicated, may hold values from 0.1 to 1.9
- per_head_bias: float32 [2048], replicated, may hold values from -1.8 to 1.8
- mixer_output_weight: bfloat16 [2048, 2048], P('ep'), may hold values from -0.125 to 0.125
- mixer_norm_gain: float32 [2048], replicated, may hold values from 0.1 to 1.9
- mixer_norm_bias: float32 [2048], replicated, may hold values from -1.8 to 1.8
- expert_norm_gain: float32 [2048], replicated, may hold values from 0.1 to 1.9
- expert_norm_bias: float32 [2048], replicated, may hold values from -1.8 to 1.8
- routes: int32 [128, 4], P(('grp', 'ep')), parts along dimension 0, may hold values from 0 to 15, all different within a row; in each aligned block of 4 rows (0 to 3, 4 to 7, ...) at most 2 rows name the same one
- routing_weight: float32 [128, 4], P(('grp', 'ep')), parts along dimension 0, may hold values from 0.1 to 1
- expert_gate_weight: bfloat16 [16, 2048, 512], P('ep'), may hold values from -0.125 to 0.125
- expert_up_weight: bfloat16 [16, 2048, 512], P('ep'), may hold values from -0.125 to 0.125
- expert_down_weight: bfloat16 [16, 512, 2048], P('ep'), may hold values from -0.25 to 0.25
Outputs:
- result: bfloat16 [128, 2048], P(('grp', 'ep')), parts along dimension 0
- next_state: float32 [128, 32, 64, 64], P(('grp', 'ep')), parts along dimension 0
There are 2 independent parts, one for each index of `grp`. A program takes and returns all parts, laid end to end along the dimension named above; an argument that names none is the same for every part. Nothing has to cross between parts.
Inputs may be any that keep to these rules, and one draw needn't show every extreme that they name: `routes`: A row names 4 different experts. Among the rows of one device no expert is named more than 2 times, and in some device one expert is named exactly 2 times; every expert is named somewhere.
All inputs are finite; a program needn't handle non-finite values.
Results may differ from a plain program's by a relative error of at most 0.0081.
Values may be sent and summed in bfloat16 or wider, within the bound.
A program may use at most 128 MiB of HBM per device.

v0:
```python
import jax
import jax.numpy as jnp
from jax import lax
from jax.sharding import PartitionSpec as P


def layer_norm(values_in, gain_vec, bias_vec):
    row_mean = jnp.mean(values_in, -1, keepdims=True)
    centered = values_in - row_mean
    row_var = jnp.mean(centered * centered, -1, keepdims=True)
    return centered * lax.rsqrt(row_var + 1e-05) * gain_vec + bias_vec


def recurrent_readout(
    tokens,
    prior_state,
    receptance_rows,
    key_rows,
    value_rows,
    decay_lowrank_first,
    decay_lowrank_second,
    decay_channel_offset,
    correction_lowrank_first,
    correction_lowrank_second,
    correction_offset,
    gate_lowrank_first,
    gate_lowrank_second,
    key_rate_blend,
    self_token_scale,
    per_head_gain,
    per_head_bias,
):
    row_count = tokens.shape[0]
    head_count = prior_state.shape[1]
    head_size = prior_state.shape[2]
    squash = jnp.tanh(
        jnp.dot(tokens, decay_lowrank_first, preferred_element_type=jnp.float32)
    ).astype(jnp.bfloat16)
    pre_decay = decay_channel_offset + jnp.dot(
        squash, decay_lowrank_second, preferred_element_type=jnp.float32
    )
    decay_rate = jnp.exp(-jnp.exp(-jax.nn.softplus(-pre_decay) - 0.5))
    low_learn = jnp.dot(
        tokens, correction_lowrank_first, preferred_element_type=jnp.float32
    ).astype(jnp.bfloat16)
    learn_rate = jax.nn.sigmoid(
        correction_offset
        + jnp.dot(low_learn, correction_lowrank_second, preferred_element_type=jnp.float32)
    )
    opened = jax.nn.sigmoid(
        jnp.dot(tokens, gate_lowrank_first, preferred_element_type=jnp.float32)
    ).astype(jnp.bfloat16)
    gating = jnp.dot(opened, gate_lowrank_second, preferred_element_type=jnp.float32)

    def by_head(flat_arr):
        return flat_arr.reshape(row_count, head_count, head_size)

    scaled = by_head(key_rows)
    unit_key = scaled * lax.rsqrt(jnp.sum(scaled * scaled, -1, keepdims=True) + 1e-06)
    written_key = by_head(key_rows * (1.0 + (learn_rate - 1.0) * key_rate_blend))
    receptance_by_head = by_head(receptance_rows)
    value_by_head = by_head(value_rows)
    removed = jnp.einsum("nhvk,nhk->nhv", prior_state, unit_key, precision=lax.Precision.HIGHEST)
    next_state = (
        prior_state * by_head(decay_rate)[:, :, None, :]
        - removed[..., None] * (unit_key * by_head(learn_rate))[:, :, None, :]
        + value_by_head[..., None] * written_key[:, :, None, :]
    )
    readout = jnp.einsum(
        "nhvk,nhk->nhv", next_state, receptance_by_head, precision=lax.Precision.HIGHEST
    )
    head_mean = jnp.mean(readout, -1, keepdims=True)
    head_dev = readout - head_mean
    head_var = jnp.mean(head_dev * head_dev, -1, keepdims=True)
    normed = (head_dev * lax.rsqrt(head_var + 0.00064)).reshape(
        row_count, -1
    ) * per_head_gain + per_head_bias
    self_token_term = (
        jnp.sum(receptance_by_head * written_key * self_token_scale, -1, keepdims=True)
        * value_by_head
    )
    mixer_result = ((normed + self_token_term.reshape(row_count, -1)) * gating).astype(jnp.bfloat16)
    return (mixer_result, next_state)


def body(
    tokens,
    prior_state,
    receptance_matrix,
    key_matrix,
    value_matrix,
    decay_lowrank_first,
    decay_lowrank_second,
    decay_channel_offset,
    correction_lowrank_first,
    correction_lowrank_second,
    correction_offset,
    gate_lowrank_first,
    gate_lowrank_second,
    key_rate_blend,
    self_token_scale,
    per_head_gain,
    per_head_bias,
    mixer_output_weight,
    mixer_norm_gain,
    mixer_norm_bias,
    expert_norm_gain,
    expert_norm_bias,
    routes,
    routing_weight,
    expert_gate_weight,
    expert_up_weight,
    expert_down_weight,
):
    own_rows = tokens.shape[0]
    mix_width = receptance_matrix.shape[1]
    columns = lax.all_to_all(tokens, "ep", split_axis=1, concat_axis=0, tiled=True)
    segment = columns
    joined = lax.psum_scatter(
        jnp.concatenate(
            [
                jnp.dot(segment, weight_mat, preferred_element_type=jnp.float32)
                for weight_mat in (receptance_matrix, key_matrix, value_matrix)
            ],
            1,
        ),
        "ep",
        scatter_dimension=0,
        tiled=True,
    )
    receptance_rows = joined[:, :mix_width]
    key_rows = joined[:, mix_width : 2 * mix_width]
    value_rows = joined[:, 2 * mix_width :]
    mixer_result, next_state = recurrent_readout(
        tokens,
        prior_state,
        receptance_rows,
        key_rows,
        value_rows,
        decay_lowrank_first,
        decay_lowrank_second,
        decay_channel_offset,
        correction_lowrank_first,
        correction_lowrank_second,
        correction_offset,
        gate_lowrank_first,
        gate_lowrank_second,
        key_rate_blend,
        self_token_scale,
        per_head_gain,
        per_head_bias,
    )
    mixer_cols = lax.all_to_all(mixer_result, "ep", split_axis=1, concat_axis=0, tiled=True)
    segment = mixer_cols
    mixed = lax.psum_scatter(
        jnp.dot(segment, mixer_output_weight, preferred_element_type=jnp.float32),
        "ep",
        scatter_dimension=0,
        tiled=True,
    )
    hidden = layer_norm(
        tokens.astype(jnp.float32) + mixed, mixer_norm_gain, mixer_norm_bias
    ).astype(jnp.bfloat16)
    model_width = hidden.shape[1]
    top_count = routes.shape[1]
    expert_count = lax.axis_size("ep")
    capacity = max(2, 2 * own_rows * top_count // expert_count)
    flat_ids = routes.reshape(-1)
    onehot = (flat_ids[:, None] == jnp.arange(expert_count, dtype=jnp.int32)[None, :]).astype(
        jnp.int32
    )
    earlier = jnp.cumsum(onehot, 0) - onehot
    slot_rank = jnp.sum(earlier * onehot, 1)
    target = flat_ids * capacity + slot_rank
    dispatch = (
        target[:, None] == jnp.arange(expert_count * capacity, dtype=jnp.int32)[None, :]
    ).astype(jnp.bfloat16)
    repeated = jnp.repeat(hidden, top_count, axis=0)
    outgoing = lax.dot_general(
        dispatch, repeated, (((0,), (0,)), ((), ())), preferred_element_type=jnp.float32
    ).astype(jnp.bfloat16)
    outgoing = outgoing.reshape(expert_count, capacity, model_width)
    arrived = lax.all_to_all(outgoing, "ep", split_axis=0, concat_axis=0, tiled=True)
    sources, slot_count, width_in = arrived.shape
    flat_in = arrived.reshape(sources * slot_count, width_in)
    gate_val = jnp.dot(flat_in, expert_gate_weight[0], preferred_element_type=jnp.float32)
    up_val = jnp.dot(flat_in, expert_up_weight[0], preferred_element_type=jnp.float32)
    inner = (jax.nn.silu(gate_val) * up_val).astype(jnp.bfloat16)
    produced = jnp.dot(inner, expert_down_weight[0], preferred_element_type=jnp.float32).astype(
        jnp.bfloat16
    )
    returned = lax.all_to_all(
        produced.reshape(sources, slot_count, width_in),
        "ep",
        split_axis=0,
        concat_axis=0,
        tiled=True,
    )
    picked = jnp.dot(
        dispatch,
        returned.reshape(expert_count * capacity, model_width),
        preferred_element_type=jnp.float32,
    )
    share = routing_weight / jnp.sum(routing_weight, -1, keepdims=True)
    combined = jnp.sum(picked.reshape(own_rows, top_count, model_width) * share[..., None], 1)
    result = layer_norm(
        hidden.astype(jnp.float32) + combined, expert_norm_gain, expert_norm_bias
    ).astype(jnp.bfloat16)
    return (result, next_state)


def solution(mesh):
    in_specs = (
        P(("grp", "ep"), None),
        P(("grp", "ep"), None, None, None),
        P("ep", None),
        P("ep", None),
        P("ep", None),
        P(),
        P(),
        P(),
        P(),
        P(),
        P(),
        P(),
        P(),
        P(),
        P(),
        P(),
        P(),
        P("ep", None),
        P(),
        P(),
        P(),
        P(),
        P(("grp", "ep"), None),
        P(("grp", "ep"), None),
        P("ep", None, None),
        P("ep", None, None),
        P("ep", None, None),
    )
    out_specs = (P(("grp", "ep"), None), P(("grp", "ep"), None, None, None))
    return jax.shard_map(body, mesh=mesh, in_specs=in_specs, out_specs=out_specs, check_vma=False)
```

profile of v0, /device:TPU:0, one launch (start us, length us, event | category | flops | bytes accessed | tf_op | source)
XLA Modules:
  0.0 282.7 jit_solution(14467927352405242082)
XLA Ops:
  7.2 14.1 %all_to_all.48 = bf16[4,16,128]{2,0,1:T(4,128)(2,1)S(1)} all-to-all(bf16[4,16,128]{2,0,1:T(4,128)(2,1)} %bitcast.64), channel_id=1, replica_groups=mesh['grp'=2,'ep'=16] {'ep'}, dimensions={1} | all-to-all | bytes 32768 | tf_op jit(solution)/shard_map/all_to_all | solution.py:117
  21.3 1.3 fusion.52
  22.6 1.3 fusion.53
  24.1 1.2 pad_maximum_fusion
  28.4 90.4 %all-reduce.5.cloned.1.call-done = f32[64,6144]{1,0:T(8,128)} async-done(((f32[64,6144]{1,0:T(8,128)}), f32[64,6144]{1,0:T(8,128)}) %all-reduce.5.cloned.1.call-update) | async-done | bytes 1572880
  118.7 1.0 add_multiply_fusion
  120.5 8.5 %fusion.55 = f32[4,32,1,64]{3,2,1,0:T(1,128)S(1)} fusion(f32[4,32,64,1]{2,3,1,0:T(1,128)S(1)} %bitcast.70, f32[4,32,64,64]{3,2,1,0:T(8,128)} %param.28), kind=kOutput, calls=%fused_computation.87 | convolution fusion | flops 6291456 | bytes 2162688 | tf_op jit(solution)/shard_map/nhvk,nhk->nhv/dot_general | solution.py:63
  129.0 2.8 multiply_add_fusion
  131.9 6.6 %fusion.56 = f32[4,32,1,64]{3,2,1,0:T(1,128)S(1)} fusion(f32[4,32,64,64]{3,2,1,0:T(8,128)S(1)} %multiply_add_fusion, f32[4,32,64,1]{2,3,1,0:T(1,128)S(1)} %bitcast.69), kind=kOutput, calls=%fused_computation.88 | convolution fusion | flops 6291456 | bytes 2162688 | tf_op jit(solution)/shard_map/nhvk,nhk->nhv/dot_general | solution.py:69
  139.2 1.0 fusion.21
  140.2 3.6 %all-to-all-start.1 = ((bf16[4,16,128]{2,0,1:T(4,128)(2,1)}), bf16[4,16,128]{2,0,1:T(4,128)(2,1)S(1)}, u32[]{:S(2)}, u32[]{:S(2)}) async-start(bf16[4,16,128]{2,0,1:T(4,128)(2,1)} %fusion.21), calls=%async_computation.1 | async-start | bytes 32768 | tf_op jit(solution)/shard_map/all_to_all | solution.py:153
  144.6 5.7 %all-to-all-done.1 = bf16[4,16,128]{2,0,1:T(4,128)(2,1)S(1)} async-done(((bf16[4,16,128]{2,0,1:T(4,128)(2,1)}), bf16[4,16,128]{2,0,1:T(4,128)(2,1)S(1)}, u32[]{:S(2)}, u32[]{:S(2)}) %all-to-all-start.1) | async-done | bytes 16416 | tf_op jit(solution)/shard_map/all_to_all | solution.py:153
  150.3 2.1 fusion.57
  152.6 87.9 %all-reduce.7.cloned.1.call-done = f32[64,2048]{1,0:T(8,128)} async-done(((f32[64,2048]{1,0:T(8,128)}), f32[64,2048]{1,0:T(8,128)}) %all-reduce.7.cloned.1.call-update) | async-done | bytes 524304
  240.5 1.0 fusion.48
  241.5 1.0 multiply_reduce_fusion.4
  242.6 0.9 add_convert_fusion.1
  244.6 5.2 %all-to-all-start.2 = ((bf16[16,2,2048]{2,1,0:T(2,128)(2,1)}), bf16[16,2,2048]{2,1,0:T(2,128)(2,1)S(1)}, u32[]{:S(2)}, u32[]{:S(2)}) async-start(bf16[16,2,2048]{2,1,0:T(2,128)(2,1)} %reshape.150), calls=%async_computation.2 | async-start | bytes 262144 | tf_op jit(solution)/shard_map/all_to_all | solution.py:183
  249.9 7.8 %all-to-all-done.2 = bf16[16,2,2048]{2,1,0:T(2,128)(2,1)S(1)} async-done(((bf16[16,2,2048]{2,1,0:T(2,128)(2,1)}), bf16[16,2,2048]{2,1,0:T(2,128)(2,1)S(1)}, u32[]{:S(2)}, u32[]{:S(2)}) %all-to-all-start.2) | async-done | bytes 131104 | tf_op jit(solution)/shard_map/all_to_all | solution.py:183
  257.7 2.0 fusion.10
  259.8 2.5 convolution_convert_fusion
  262.3 0.8 reshape.152
  263.1 3.5 %all-to-all-start.3 = ((bf16[16,2,2048]{2,1,0:T(2,128)(2,1)}), bf16[16,2,2048]{2,1,0:T(2,128)(2,1)S(1)}, u32[]{:S(2)}, u32[]{:S(2)}) async-start(bf16[16,2,2048]{2,1,0:T(2,128)(2,1)} %reshape.152), calls=%async_computation.3 | async-start | bytes 262144 | tf_op jit(solution)/shard_map/all_to_all | solution.py:192
  266.8 7.7 %all-to-all-done.3 = bf16[16,2,2048]{2,1,0:T(2,128)(2,1)S(1)} async-done(((bf16[16,2,2048]{2,1,0:T(2,128)(2,1)}), bf16[16,2,2048]{2,1,0:T(2,128)(2,1)S(1)}, u32[]{:S(2)}, u32[]{:S(2)}) %all-to-all-start.3) | async-done | bytes 131104 | tf_op jit(solution)/shard_map/all_to_all | solution.py:192
  (103 shorter events, 7.8 us)
Async XLA Ops:
  7.2 252.6 %copy-start = (bf16[1,512,2048]{2,1,0:T(8,128)(2,1)S(1)}, bf16[1,512,2048]{2,1,0:T(8,128)(2,1)}, u32[]{:S(2)}) copy-start(bf16[1,512,2048]{2,1,0:T(8,128)(2,1)} %param.53) | copy-start | bytes 6291460
  7.2 16.6 %copy-start.6 = (bf16[128,2048]{1,0:T(8,128)(2,1)S(1)}, bf16[128,2048]{1,0:T(8,128)(2,1)}, u32[]{:S(2)}) copy-start(bf16[128,2048]{1,0:T(8,128)(2,1)} %param.31) | copy-start | bytes 1572868
  7.2 111.5 %all-reduce.5.cloned.1.call-start = ((), (), s32[]{:S(2)}) async-start(), calls=%async_computation.4 | async-start | bytes 3145728
  24.1 1.9 copy-start.9
  25.4 93.4 %copy-start.16 = (f32[2048]{0:T(1024)S(1)}, f32[2048]{0:T(1024)}, u32[]{:S(2)}) copy-start(f32[2048]{0:T(1024)} %param.40) | copy-start | bytes 24580
  120.5 8.5 %copy-start.1 = (f32[4,32,64,64]{3,2,1,0:T(8,128)S(1)}, f32[4,32,64,64]{3,2,1,0:T(8,128)}, u32[]{:S(2)}) copy-start(f32[4,32,64,64]{3,2,1,0:T(8,128)} %param.28) | copy-start | bytes 6291460
  131.8 6.7 %copy-start.2 = (f32[4,32,64,64]{3,2,1,0:T(8,128)}, f32[4,32,64,64]{3,2,1,0:T(8,128)S(1)}, u32[]{:S(2)}) copy-start(f32[4,32,64,64]{3,2,1,0:T(8,128)S(1)} %multiply_add_fusion) | copy-start | bytes 6291460
  131.8 7.2 %copy-start.11 = (f32[32,64]{1,0:T(8,128)S(1)}, f32[32,64]{1,0:T(8,128)}, u32[]{:S(2)}) copy-start(f32[32,64]{1,0:T(8,128)} %param.41) | copy-start | bytes 24580
  131.8 7.4 %copy-start.4 = (bf16[128,2048]{1,0:T(8,128)(2,1)S(1)}, bf16[128,2048]{1,0:T(8,128)(2,1)}, u32[]{:S(2)}) copy-start(bf16[128,2048]{1,0:T(8,128)(2,1)} %param.39) | copy-start | bytes 1572868
  131.8 7.4 %copy-start.5 = (bf16[2048,128]{1,0:T(8,128)(2,1)S(1)}, bf16[2048,128]{1,0:T(8,128)(2,1)}, u32[]{:S(2)}) copy-start(bf16[2048,128]{1,0:T(8,128)(2,1)} %param.38) | copy-start | bytes 1572868
  131.8 7.4 %copy-start.14 = (f32[2048]{0:T(1024)S(1)}, f32[2048]{0:T(1024)}, u32[]{:S(2)}) copy-start(f32[2048]{0:T(1024)} %param.43) | copy-start | bytes 24580
  131.8 7.4 %copy-start.15 = (f32[2048]{0:T(1024)S(1)}, f32[2048]{0:T(1024)}, u32[]{:S(2)}) copy-start(f32[2048]{0:T(1024)} %param.42) | copy-start | bytes 24580
  138.4 13.9 %copy-start.25 = (s32[16]{0:T(128)S(1)}, s32[16]{0:T(128)}, u32[]{:S(2)}) copy-start(s32[16]{0:T(128)} %eq.50) | copy-start | bytes 196
  138.4 104.1 %copy-start.21 = (f32[2048]{0:T(1024)S(1)}, f32[2048]{0:T(1024)}, u32[]{:S(2)}) copy-start(f32[2048]{0:T(1024)} %param.46) | copy-start | bytes 24580
  138.5 104.1 %copy-start.22 = (f32[2048]{0:T(1024)S(1)}, f32[2048]{0:T(1024)}, u32[]{:S(2)}) copy-start(f32[2048]{0:T(1024)} %param.45) | copy-start | bytes 24580
  139.0 110.8 %copy-start.19 = (f32[4,4]{1,0:T(4,128)S(1)}, f32[4,4]{1,0:T(4,128)}, u32[]{:S(2)}) copy-start(f32[4,4]{1,0:T(4,128)} %param.50) | copy-start | bytes 196
  140.2 10.1 %all-to-all-start.1 = ((bf16[4,16,128]{2,0,1:T(4,128)(2,1)}), bf16[4,16,128]{2,0,1:T(4,128)(2,1)S(1)}, u32[]{:S(2)}, u32[]{:S(2)}) async-start(bf16[4,16,128]{2,0,1:T(4,128)(2,1)} %fusion.21), calls=%async_computation.1 | async-start | bytes 32768 | tf_op jit(solution)/shard_map/all_to_all | solution.py:153
  143.8 96.7 %all-reduce.7.cloned.1.call-start = ((), (), s32[]{:S(2)}) async-start(), calls=%async_computation.5 | async-start | bytes 1048576
  244.6 13.1 %all-to-all-start.2 = ((bf16[16,2,2048]{2,1,0:T(2,128)(2,1)}), bf16[16,2,2048]{2,1,0:T(2,128)(2,1)S(1)}, u32[]{:S(2)}, u32[]{:S(2)}) async-start(bf16[16,2,2048]{2,1,0:T(2,128)(2,1)} %reshape.150), calls=%async_computation.2 | async-start | bytes 262144 | tf_op jit(solution)/shard_map/all_to_all | solution.py:183
  259.8 6.8 %copy-start.20 = (f32[4,4]{1,0:T(4,128)S(1)}, f32[4,4]{1,0:T(4,128)}, u32[]{:S(2)}) copy-start(f32[4,4]{1,0:T(4,128)} %param.50) | copy-start | bytes 196
  259.8 7.0 %copy-start.18 = (s32[4,4]{1,0:T(4,128)S(1)}, s32[4,4]{1,0:T(4,128)}, u32[]{:S(2)}) copy-start(s32[4,4]{1,0:T(4,128)} %param.49) | copy-start | bytes 196
  259.8 15.4 %copy-start.23 = (f32[2048]{0:T(1024)S(1)}, f32[2048]{0:T(1024)}, u32[]{:S(2)}) copy-start(f32[2048]{0:T(1024)} %param.48) | copy-start | bytes 24580
  259.8 15.4 %copy-start.24 = (f32[2048]{0:T(1024)S(1)}, f32[2048]{0:T(1024)}, u32[]{:S(2)}) copy-start(f32[2048]{0:T(1024)} %param.47) | copy-start | bytes 24580
  263.1 11.4 %all-to-all-start.3 = ((bf16[16,2,2048]{2,1,0:T(2,128)(2,1)}), bf16[16,2,2048]{2,1,0:T(2,128)(2,1)S(1)}, u32[]{:S(2)}, u32[]{:S(2)}) async-start(bf16[16,2,2048]{2,1,0:T(2,128)(2,1)} %reshape.152), calls=%async_computation.3 | async-start | bytes 262144 | tf_op jit(solution)/shard_map/all_to_all | solution.py:192
  (8 other events, 12.1 us)
Sparse Core Ops, SparseCore 0:
  25.5 93.1 all-reduce.4
  152.5 87.9 all-reduce.6
where the time goes:
time: 284 us; the launch traced here: 283 us
  waiting for transfers between devices  200 us (70%)
  matrix products  26.8 us (9%)
  between operations  15.2 us (5%)
  blocking collectives  14.1 us (5%)
  starting transfers between devices  12.4 us (4%)
  other arithmetic  10.8 us (4%)
  local copies, waits for them, and re-layouts  3.99 us (1%)
    unnamed x4, waiting for transfers between devices  178 us
    all_to_all x1, blocking collectives, body(): lax.all_to_all(tokens, 'ep', split_axis=1, concat_axis=0, tiled=True)  14.1 us
    dot_general x1, matrix products, recurrent_readout(): jnp.einsum('nhvk,nhk->nhv', prior_state, unit_key, precision=lax.Precisio...  8.52 us
    all_to_all x1, waiting for transfers between devices, body(): lax.all_to_all(outgoing, 'ep', split_axis=0, concat_axis=0, tiled=True)  7.77 us
    all_to_all x1, waiting for transfers between devices, body(): lax.all_to_all(produced.reshape(sources, slot_count, width_in), 'ep', spl...  7.7 us
    dot_general x1, matrix products, recurrent_readout(): jnp.einsum('nhvk,nhk->nhv', next_state, receptance_by_head, precision=lax...  6.58 us
    all_to_all x1, waiting for transfers between devices, body(): lax.all_to_all(mixer_result, 'ep', split_axis=1, concat_axis=0, tiled=True)  5.71 us
  transfers between devices with their start and end apart: 5, of which 5 were waited for; matrix products, arithmetic and copies ran while one was open for 1% of the time, Pallas kernels for 0%

commit v1 on v0

v1 whole, which is shorter than its diff:
```python
import functools

import jax
import jax.numpy as jnp
from jax import lax
from jax.experimental import pallas as pl
from jax.experimental.pallas import tpu as pltpu
from jax.sharding import PartitionSpec as P

F32 = jnp.float32
BF16 = jnp.bfloat16
MESH = pl.DeviceIdType.MESH
LANES = 128


def layer_norm(values_in, gain_vec, bias_vec):
    row_mean = jnp.mean(values_in, -1, keepdims=True)
    centered = values_in - row_mean
    row_var = jnp.mean(centered * centered, -1, keepdims=True)
    return centered * lax.rsqrt(row_var + 1e-05) * gain_vec + bias_vec


def matmul(left, right):
    return jnp.dot(left, right, preferred_element_type=F32)


def sigmoid(u):
    return 1.0 / (1.0 + jnp.exp(-u))


def kernel(
    n,
    capacity,
    routes,
    routing_weight,
    tokens_hbm,
    state_hbm,
    key_hbm,
    value_hbm,
    receptance_hbm,
    mixer_out_hbm,
    decay_first_hbm,
    decay_second_hbm,
    learn_first_hbm,
    learn_second_hbm,
    gate_first_hbm,
    gate_second_hbm,
    decay_offset_hbm,
    learn_offset_hbm,
    blend_hbm,
    head_gain_hbm,
    head_bias_hbm,
    mixer_gain_hbm,
    mixer_bias_hbm,
    expert_gain_hbm,
    expert_bias_hbm,
    self_scale_hbm,
    expert_gate_hbm,
    expert_up_hbm,
    expert_down_hbm,
    result,
    next_hbm,
    tokens,
    state,
    weights,
    decay_first,
    decay_second,
    learn_first,
    learn_second,
    gate_first,
    gate_second,
    vectors,
    self_scale,
    expert_gate,
    expert_up,
    expert_down,
    token_send,
    token_recv,
    part_send,
    part_recv,
    slot_send,
    slot_recv,
    back_send,
    back_recv,
    heads,
    value_flat,
    mixed_rows,
    load_sem,
    state_in_sem,
    state_out_sem,
    weight_sem,
    weight_send_sem,
    weight_recv_sem,
    token_send_sem,
    token_recv_sem,
    part_send_sem,
    part_recv_sem,
    slot_send_sem,
    slot_recv_sem,
    back_send_sem,
    back_recv_sem,
):
    me = lax.axis_index("ep")
    chips = n // 2
    chip, core = me // 2, lax.rem(me, 2)
    partner = chip * 2 + (1 - core)
    rows, width = tokens.shape
    head_count, head_size = self_scale.shape
    matrix_rows = key_hbm.shape[0]
    chip_rows = 2 * matrix_rows
    block = token_recv.shape[-1]

    if chip_rows < block:
        weights[...] = jnp.zeros_like(weights)

    barrier = pltpu.get_barrier_semaphore()

    def greet(step, carry):
        pl.semaphore_signal(
            barrier, inc=1, device_id={"ep": lax.rem(me + step, n)}, device_id_type=MESH
        )
        return carry

    lax.fori_loop(1, n, greet, 0)

    loads = [
        (tokens_hbm, tokens),
        (decay_first_hbm, decay_first),
        (learn_first_hbm, learn_first),
        (gate_first_hbm, gate_first),
        (decay_second_hbm, decay_second),
        (learn_second_hbm, learn_second),
        (gate_second_hbm, gate_second),
        (decay_offset_hbm, vectors.at[0]),
        (learn_offset_hbm, vectors.at[1]),
        (blend_hbm, vectors.at[2]),
        (head_gain_hbm, vectors.at[3]),
        (head_bias_hbm, vectors.at[4]),
        (mixer_gain_hbm, vectors.at[5]),
        (mixer_bias_hbm, vectors.at[6]),
        (expert_gain_hbm, vectors.at[7]),
        (expert_bias_hbm, vectors.at[8]),
        (self_scale_hbm, self_scale),
        (expert_gate_hbm.at[0], expert_gate),
        (expert_up_hbm.at[0], expert_up),
        (expert_down_hbm.at[0], expert_down),
    ]
    copies = [
        pltpu.make_async_copy(src, dst, load_sem.at[i]) for i, (src, dst) in enumerate(loads)
    ]
    row_at = pl.multiple_of(lax.rem(chip * chip_rows, block) + core * matrix_rows, matrix_rows)
    other_at = pl.multiple_of(
        lax.rem(chip * chip_rows, block) + (1 - core) * matrix_rows, matrix_rows
    )
    sources = (key_hbm, value_hbm, receptance_hbm, mixer_out_hbm)
    own_weight = [
        pltpu.make_async_copy(src, weights.at[i, pl.ds(row_at, matrix_rows), :], weight_sem.at[i])
        for i, src in enumerate(sources)
    ]
    push_weight = [
        pltpu.make_async_remote_copy(
            src_ref=src,
            dst_ref=weights.at[i, pl.ds(row_at, matrix_rows), :],
            send_sem=weight_send_sem.at[i],
            recv_sem=weight_recv_sem.at[i],
            device_id={"ep": partner},
            device_id_type=MESH,
        )
        for i, src in enumerate(sources)
    ]
    pull_weight = [
        pltpu.make_async_remote_copy(
            src_ref=src,
            dst_ref=weights.at[i, pl.ds(other_at, matrix_rows), :],
            send_sem=weight_send_sem.at[i],
            recv_sem=weight_recv_sem.at[i],
            device_id={"ep": partner},
            device_id_type=MESH,
        )
        for i, src in enumerate(sources)
    ]
    for copy in copies[:7]:
        copy.start()
    for copy in own_weight[:3]:
        copy.start()
    for copy in copies[7:17]:
        copy.start()
    state_in = [
        pltpu.make_async_copy(state_hbm.at[t], state.at[t], state_in_sem.at[t]) for t in range(rows)
    ]
    for copy in state_in:
        copy.start()
    own_weight[3].start()
    for copy in copies[17:]:
        copy.start()

    def chip_copy(send_ref, recv_ref, send_sem, recv_sem, to, source):
        return pltpu.make_async_remote_copy(
            src_ref=send_ref.at[to],
            dst_ref=recv_ref.at[source],
            send_sem=send_sem.at[to],
            recv_sem=recv_sem.at[source],
            device_id={"ep": to * 2 + core},
            device_id_type=MESH,
        )

    def device_copy(send_ref, recv_ref, send_sem, recv_sem, to, source):
        return pltpu.make_async_remote_copy(
            src_ref=send_ref.at[to],
            dst_ref=recv_ref.at[source],
            send_sem=send_sem.at[to],
            recv_sem=recv_sem.at[source],
            device_id={"ep": to},
            device_id_type=MESH,
        )

    def exchange(make, count, own):
        def send(step, carry):
            make(lax.rem(own + step, count), own).start()
            return carry

        def finish(step, carry):
            other = lax.rem(own + step, count)
            make(other, other).wait_recv()
            return carry

        def drain(step, carry):
            make(lax.rem(own + step, count), own).wait_send()
            return carry

        return (
            lambda: lax.fori_loop(1, count, send, 0),
            lambda: lax.fori_loop(1, count, finish, 0),
            lambda: lax.fori_loop(1, count, drain, 0),
        )

    def among_chips(send_ref, recv_ref, send_sem, recv_sem):
        return exchange(
            functools.partial(chip_copy, send_ref, recv_ref, send_sem, recv_sem), chips, chip
        )

    def among_devices(send_ref, recv_ref, send_sem, recv_sem):
        return exchange(
            functools.partial(device_copy, send_ref, recv_ref, send_sem, recv_sem), n, me
        )

    def spread(phase, flat):
        send_ref, recv_ref = token_send.at[phase], token_recv.at[phase]
        for j in range(chips):
            at = j * chip_rows // block * block
            send_ref[j] = flat[:, at : at + block]
        recv_ref[chip] = send_ref[chip]
        return among_chips(
            send_ref, recv_ref, token_send_sem.at[phase], token_recv_sem.at[phase]
        )

    def gathered(phase):
        return jnp.concatenate([token_recv[phase, j] for j in range(chips)], 0).astype(BF16)

    def partial_product(i, segment):
        own_weight[i].wait()
        pull_weight[i].wait_recv()
        product = matmul(segment, weights[i])
        for j in range(chips):
            part_send[i, j] = product[j * rows : (j + 1) * rows].astype(BF16)
        part_recv[i, chip] = part_send[i, chip]
        return among_chips(
            part_send.at[i], part_recv.at[i], part_send_sem.at[i], part_recv_sem.at[i]
        )

    def summed(i):
        total = part_recv[i, 0].astype(F32)
        for j in range(1, chips):
            total = total + part_recv[i, j].astype(F32)
        return total

    copies[0].wait()
    own = tokens[...]
    own_wide = own.astype(F32)
    token_go, token_wait, token_drain = spread(0, own_wide)
    pl.semaphore_wait(barrier, n - 1)
    token_go()
    for copy in push_weight:
        copy.start()

    for copy in copies[1:17]:
        copy.wait()
    squash = jnp.tanh(matmul(own, decay_first[...])).astype(BF16)
    pre_decay = vectors[0] + matmul(squash, decay_second[...])
    softplus = jnp.maximum(-pre_decay, 0.0) + jnp.log(1.0 + jnp.exp(-jnp.abs(pre_decay)))
    decay_rate = jnp.exp(-jnp.exp(-softplus - 0.5))
    low = matmul(own, learn_first[...]).astype(BF16)
    learn_rate = sigmoid(vectors[1] + matmul(low, learn_second[...]))
    key_factor = 1.0 + (learn_rate - 1.0) * vectors[2]
    opened = sigmoid(matmul(own, gate_first[...])).astype(BF16)
    gating = matmul(opened, gate_second[...])

    def by_head(i, flat):
        for h in range(head_count):
            heads[i, h * rows : (h + 1) * rows, :] = flat[:, h * head_size : (h + 1) * head_size]

    by_head(0, decay_rate)
    by_head(1, learn_rate)
    by_head(2, key_factor)

    token_wait()
    segment = gathered(0)
    parts = []
    for i in range(3):
        part = partial_product(i, segment)
        part[0]()
        parts.append(part)
    parts[0][1]()
    by_head(3, summed(0))
    parts[1][1]()
    value_flat[...] = summed(1)
    parts[2][1]()
    by_head(4, summed(2))

    mask_shape = (head_count, width)
    in_head = (
        lax.broadcasted_iota(jnp.int32, mask_shape, 1) // head_size
        == lax.broadcasted_iota(jnp.int32, mask_shape, 0)
    )
    for t in range(rows):
        decay_t, learn_t, factor_t, key_t, rec_t = [
            heads[i, pl.ds(t, head_count, stride=rows), :] for i in range(5)
        ]
        unit_t = key_t * lax.rsqrt(jnp.sum(key_t * key_t, -1, keepdims=True) + 1e-06)
        written_t = key_t * factor_t
        change_t = unit_t * learn_t
        value_t = jnp.broadcast_to(value_flat[t : t + 1, :], mask_shape)
        probes = jnp.concatenate([unit_t, decay_t * rec_t], 0).astype(BF16)
        state_in[t].wait()
        before = state[t]
        flat_state = before.reshape(width, head_size)
        found = lax.dot_general(
            probes, flat_state.astype(BF16), (((1,), (1,)), ((), ())), preferred_element_type=F32
        )
        removed = found[:head_count]
        change_rec = jnp.sum(change_t * rec_t, -1, keepdims=True)
        written_rec = jnp.sum(written_t * rec_t, -1, keepdims=True)
        own_term = jnp.sum(rec_t * written_t * self_scale[...], -1, keepdims=True)
        readout = jnp.where(
            in_head, found[head_count:] - removed * change_rec + value_t * written_rec, 0.0
        )
        head_mean = jnp.sum(readout, -1, keepdims=True) * (1.0 / head_size)
        head_dev = jnp.where(in_head, readout - head_mean, 0.0)
        head_var = jnp.sum(head_dev * head_dev, -1, keepdims=True) * (1.0 / head_size)
        normed = head_dev * lax.rsqrt(head_var + 0.00064)
        mixed_rows[t : t + 1, :] = jnp.sum(normed, 0, keepdims=True)
        mixed_rows[rows + t : rows + t + 1, :] = jnp.sum(
            jnp.where(in_head, own_term * value_t, 0.0), 0, keepdims=True
        )
        columns = jnp.concatenate(
            [jnp.where(in_head, value_t, 0.0), jnp.where(in_head, -removed, 0.0)], 0
        ).astype(BF16)
        rank_rows = jnp.concatenate([written_t, change_t], 0).astype(BF16)
        added = lax.dot_general(
            columns, rank_rows, (((0,), (0,)), ((), ())), preferred_element_type=F32
        ).reshape(head_count, head_size, head_size)
        for h in range(head_count):
            state[t, h] = before[h] * decay_t[h : h + 1, :] + added[h]
        pltpu.make_async_copy(state.at[t], next_hbm.at[t], state_out_sem.at[t]).start()

    normed = mixed_rows[:rows] * vectors[3] + vectors[4]
    mixer_result = ((normed + mixed_rows[rows:]) * gating).astype(BF16).astype(F32)
    mixer_go, mixer_wait, mixer_drain = spread(1, mixer_result)
    mixer_go()
    mixer_wait()
    out_go, out_wait, out_drain = partial_product(3, gathered(1))
    out_go()

    top = routes.shape[1]
    slots = n * capacity

    def routing(shape, axis):
        slot = lax.broadcasted_iota(jnp.int32, shape, axis)
        expert, place = slot // capacity, lax.rem(slot, capacity)
        earlier = jnp.zeros(shape, jnp.int32)
        held, shares = [], []
        for t in range(rows):
            hit = jnp.zeros(shape, jnp.int32)
            weight = jnp.zeros(shape, F32)
            total = jnp.zeros(shape, F32)
            for k in range(top):
                same = expert == routes[t, k]
                hit = hit + jnp.where(same, 1, 0)
                weight = weight + jnp.where(same, routing_weight[t, k], 0.0)
                total = total + routing_weight[t, k]
            live = (earlier == place) & (hit > 0)
            held.append(jnp.where(live, 1.0, 0.0))
            shares.append(jnp.where(live, weight / total, 0.0))
            earlier = earlier + hit
        return held, shares

    held, _ = routing((slots, 1), 0)
    _, shares = routing((1, slots), 1)
    share = jnp.concatenate(shares, 0)
    share_high = share.astype(BF16)
    share_low = (share - share_high.astype(F32)).astype(BF16)

    out_wait()
    hidden = (
        layer_norm(own_wide + summed(3), vectors[5], vectors[6]).astype(BF16).astype(F32)
    )
    outgoing = held[0] * hidden[0:1]
    for t in range(1, rows):
        outgoing = outgoing + held[t] * hidden[t : t + 1]
    for e in range(n):
        slot_send[e] = outgoing[e * capacity : (e + 1) * capacity].astype(BF16)
    slot_recv[me] = slot_send[me]
    slot_go, slot_wait, slot_drain = among_devices(
        slot_send, slot_recv, slot_send_sem, slot_recv_sem
    )
    slot_go()
    for copy in copies[17:]:
        copy.wait()
    slot_wait()
    arrived = jnp.concatenate([slot_recv[s].astype(F32) for s in range(n)], 0).astype(BF16)
    gate_val = matmul(arrived, expert_gate[...])
    up_val = matmul(arrived, expert_up[...])
    inner = (gate_val * sigmoid(gate_val) * up_val).astype(BF16)
    produced = matmul(inner, expert_down[...])
    for s in range(n):
        back_send[s] = produced[s * capacity : (s + 1) * capacity].astype(BF16)
    back_recv[me] = back_send[me]
    back_go, back_wait, back_drain = among_devices(
        back_send, back_recv, back_send_sem, back_recv_sem
    )
    back_go()
    token_drain()
    mixer_drain()
    for part in parts:
        part[2]()
    out_drain()
    slot_drain()
    for copy in push_weight:
        copy.wait_send()
    for t in range(rows):
        pltpu.make_async_copy(state.at[t], next_hbm.at[t], state_out_sem.at[t]).wait()
    back_wait()
    returned = jnp.concatenate([back_recv[e].astype(F32) for e in range(n)], 0).astype(BF16)
    combined = matmul(share_high, returned) + matmul(share_low, returned)
    result[...] = layer_norm(hidden + combined, vectors[7], vectors[8]).astype(BF16)
    back_drain()


def body(
    tokens,
    prior_state,
    receptance_matrix,
    key_matrix,
    value_matrix,
    decay_lowrank_first,
    decay_lowrank_second,
    decay_channel_offset,
    correction_lowrank_first,
    correction_lowrank_second,
    correction_offset,
    gate_lowrank_first,
    gate_lowrank_second,
    key_rate_blend,
    self_token_scale,
    per_head_gain,
    per_head_bias,
    mixer_output_weight,
    mixer_norm_gain,
    mixer_norm_bias,
    expert_norm_gain,
    expert_norm_bias,
    routes,
    routing_weight,
    expert_gate_weight,
    expert_up_weight,
    expert_down_weight,
):
    n = lax.axis_size("ep")
    chips = n // 2
    rows, width = tokens.shape
    head_count, head_size = self_token_scale.shape
    capacity = max(2, 2 * rows * routes.shape[1] // n)
    block = max(2 * key_matrix.shape[0], LANES)
    vectors = [
        v.reshape(1, -1)
        for v in (
            decay_channel_offset,
            correction_offset,
            key_rate_blend,
            per_head_gain,
            per_head_bias,
            mixer_norm_gain,
            mixer_norm_bias,
            expert_norm_gain,
            expert_norm_bias,
        )
    ]
    anywhere = pl.BlockSpec(memory_space=pl.ANY)
    scalars = pl.BlockSpec(memory_space=pltpu.SMEM)
    dma = pltpu.SemaphoreType.DMA
    vmem = pltpu.VMEM
    operands = [
        tokens,
        prior_state,
        key_matrix,
        value_matrix,
        receptance_matrix,
        mixer_output_weight,
        decay_lowrank_first,
        decay_lowrank_second,
        correction_lowrank_first,
        correction_lowrank_second,
        gate_lowrank_first,
        gate_lowrank_second,
        *vectors,
        self_token_scale,
        expert_gate_weight,
        expert_up_weight,
        expert_down_weight,
    ]
    return tuple(
        pl.pallas_call(
            functools.partial(kernel, n, capacity),
            out_shape=(
                jax.ShapeDtypeStruct(tokens.shape, BF16),
                jax.ShapeDtypeStruct(prior_state.shape, F32),
            ),
            in_specs=[scalars, scalars] + [anywhere] * len(operands),
            out_specs=(pl.BlockSpec(memory_space=pltpu.VMEM), anywhere),
            scratch_shapes=[
                vmem(tokens.shape, BF16),
                vmem(prior_state.shape, F32),
                vmem((4, block, width), BF16),
                vmem(decay_lowrank_first.shape, BF16),
                vmem(decay_lowrank_second.shape, BF16),
                vmem(correction_lowrank_first.shape, BF16),
                vmem(correction_lowrank_second.shape, BF16),
                vmem(gate_lowrank_first.shape, BF16),
                vmem(gate_lowrank_second.shape, BF16),
                vmem((len(vectors), 1, width), F32),
                vmem(self_token_scale.shape, F32),
                vmem(expert_gate_weight.shape[1:], BF16),
                vmem(expert_up_weight.shape[1:], BF16),
                vmem(expert_down_weight.shape[1:], BF16),
                vmem((2, chips, rows, block), F32),
                vmem((2, chips, rows, block), F32),
                vmem((4, chips, rows, width), BF16),
                vmem((4, chips, rows, width), BF16),
                vmem((n, capacity, width), BF16),
                vmem((n, capacity, width), BF16),
                vmem((n, capacity, width), BF16),
                vmem((n, capacity, width), BF16),
                vmem((5, head_count * rows, head_size), F32),
                vmem((rows, width), F32),
                vmem((2 * rows, width), F32),
                dma((20,)),
                dma((rows,)),
                dma((rows,)),
                dma((4,)),
                dma((4,)),
                dma((4,)),
                dma((2, chips)),
                dma((2, chips)),
                dma((4, chips)),
                dma((4, chips)),
                dma((n,)),
                dma((n,)),
                dma((n,)),
                dma((n,)),
            ],
            compiler_params=pltpu.CompilerParams(
                collective_id=0, has_side_effects=True, vmem_limit_bytes=60 * 1024 * 1024
            ),
        )(routes, routing_weight, *operands)
    )


def solution(mesh):
    split = P(("grp", "ep"), None)
    state = P(("grp", "ep"), None, None, None)
    matrix = P("ep", None)
    expert = P("ep", None, None)
    in_specs = (
        (split, state)
        + (matrix,) * 3
        + (P(),) * 12
        + (matrix,)
        + (P(),) * 4
        + (split, split)
        + (expert,) * 3
    )
    return jax.shard_map(
        body, mesh=mesh, in_specs=in_specs, out_specs=(split, state), check_vma=False
    )
```

time: 284 us -> 57.3 us (0.20)
  waiting for transfers between devices: 200 us -> 0 us
  Pallas kernels: 0 us -> 46.2 us
  matrix products: 26.8 us -> 0 us
  between operations: 15.2 us -> 0.64 us
  blocking collectives: 14.1 us -> 0 us
  starting transfers between devices: 12.4 us -> 0 us
  other arithmetic: 10.8 us -> 0 us
  local copies, waits for them, and re-layouts: 3.99 us -> 10 us
    unnamed x4 -> x0, waiting for transfers between devices: 178 us -> none
    pallas_call x0 -> x1, Pallas kernels: none -> 46.2 us  [body(): pl.pallas_call(functools.partial(kernel, n, capacity), out_shape=(jax.Sha...]
    dot_general x13 -> x0, matrix products: 26.8 us -> none  [the longest x1 8.52 us: recurrent_readout(): jnp.einsum('nhvk,nhk->nhv', prior_state, unit_key, precision=lax.Precisio...]
    all_to_all x3 -> x0, waiting for transfers between devices: 21.2 us -> none  [the longest x1 7.77 us: body(): lax.all_to_all(outgoing, 'ep', split_axis=0, concat_axis=0, tiled=True)]
    all_to_all x1 -> x0, blocking collectives: 14.1 us -> none  [body(): lax.all_to_all(tokens, 'ep', split_axis=1, concat_axis=0, tiled=True)]
    all_to_all x3 -> x0, starting transfers between devices: 12.3 us -> none  [the longest x1 5.17 us: body(): lax.all_to_all(outgoing, 'ep', split_axis=0, concat_axis=0, tiled=True)]
    unnamed x55 -> x4, local copies, waits for them, and re-layouts: 0.75 us -> 10 us
    reduce_sum x9 -> x0, other arithmetic: 3 us -> none  [the longest x2 1.24 us: layer_norm(): row_var = jnp.mean(centered * centered, -1, keepdims=True)]
  transfers between devices with their start and end apart: 5 -> 0, of which waited for: 5 -> 0; matrix products, arithmetic and copies ran while one was open for 1% -> 0% of each run, Pallas kernels for 0% -> 0%
where the time goes in v1:
time: 57.3 us; the launch traced here: 56.9 us
  Pallas kernels  46.2 us (81%)
  local copies, waits for them, and re-layouts  10 us (17%)
  between operations  0.64 us (1%)
    pallas_call x1, Pallas kernels, body(): pl.pallas_call(functools.partial(kernel, n, capacity), out_shape=(jax.Sha...  46.2 us
    unnamed x4, local copies, waits for them, and re-layouts  10 us

profile of v1, /device:TPU:0, one launch (start us, length us, event | category | flops | bytes accessed | tf_op | source)
XLA Modules:
  0.0 56.9 jit_solution(6249580831857812881)
XLA Ops:
  0.6 2.0 %copy.29.decay_first_hbm = bf16[2048,64]{1,0:T(8,128)(2,1)} copy(bf16[2048,64]{0,1:T(8,128)(2,1)} %param.32) | data formatting | bytes 524288 | tf_op args[5]
  2.6 1.9 %copy.30.learn_first_hbm = bf16[2048,64]{1,0:T(8,128)(2,1)} copy(bf16[2048,64]{0,1:T(8,128)(2,1)} %param.35) | data formatting | bytes 524288 | tf_op args[8]
  4.5 46.2 %shard_map.266 = (bf16[4,2048]{1,0:T(4,128)(2,1)}, f32[4,32,64,64]{3,2,1,0:T(8,128)}) custom-call(s32[4,4]{1,0:T(4,128)} %routes.1, f32[4,4]{1,0:T(4,128)} %routing_weight.1, bf16[4,2048]{1,0:T(4,128)(2,1)} %tokens_hbm.1, f32[4,32,64,64]{3,2,1,0:T(8,128)} %state_hbm.1, bf16[128,2048]{1,0:T(8,128)(2,1)} %key_hbm.1, bf16[128,2048]{1,0:T(8,128)(2,1)} %value_hbm.1, ...), custom_call_target="tpu_custom_call" | custom-call | tf_op jit(solution)/shard_map/pallas_call | solution.py:522
  50.8 1.3 %copy.33 = bf16[4,2048]{1,0:T(4,128)(2,1)} copy(bf16[4,2048]{1,0:T(4,128)(2,1)} %get-tuple-element.4) | data formatting | bytes 32768
  52.1 4.8 %copy.34 = f32[4,32,64,64]{3,2,1,0:T(8,128)} copy(f32[4,32,64,64]{3,2,1,0:T(8,128)} %get-tuple-element.5) | data formatting | bytes 4194304

commit v2 on v1

--- a/solution.py
+++ b/solution.py
@@ -22,6 +22,10 @@
 
 def matmul(left, right):
     return jnp.dot(left, right, preferred_element_type=F32)
+
+
+def matmul_t(left, right):
+    return lax.dot_general(left, right, (((1,), (1,)), ((), ())), preferred_element_type=F32)
 
 
 def sigmoid(u):
@@ -52,14 +56,14 @@
     head_bias_hbm,
     mixer_gain_hbm,
     mixer_bias_hbm,
-    expert_gain_hbm,
-    expert_bias_hbm,
     self_scale_hbm,
     expert_gate_hbm,
     expert_up_hbm,
     expert_down_hbm,
-    result,
-    next_hbm,
+    next_state,
+    returned,
+    hidden_out,
+    share_out,
     tokens,
     state,
     weights,
@@ -81,13 +85,14 @@
     slot_send,
     slot_recv,
     back_send,
-    back_recv,
     heads,
     value_flat,
     mixed_rows,
+    columns,
+    rank_rows,
+    back_recv,
     load_sem,
     state_in_sem,
-    state_out_sem,
     weight_sem,
     weight_send_sem,
     weight_recv_sem,
@@ -138,8 +143,6 @@
         (head_bias_hbm, vectors.at[4]),
         (mixer_gain_hbm, vectors.at[5]),
         (mixer_bias_hbm, vectors.at[6]),
-        (expert_gain_hbm, vectors.at[7]),
-        (expert_bias_hbm, vectors.at[8]),
         (self_scale_hbm, self_scale),
         (expert_gate_hbm.at[0], expert_gate),
         (expert_up_hbm.at[0], expert_up),
@@ -183,7 +186,7 @@
         copy.start()
     for copy in own_weight[:3]:
         copy.start()
-    for copy in copies[7:17]:
+    for copy in copies[7:15]:
         copy.start()
     state_in = [
         pltpu.make_async_copy(state_hbm.at[t], state.at[t], state_in_sem.at[t]) for t in range(rows)
@@ -191,7 +194,7 @@
     for copy in state_in:
         copy.start()
     own_weight[3].start()
-    for copy in copies[17:]:
+    for copy in copies[15:]:
         copy.start()
 
     def chip_copy(send_ref, recv_ref, send_sem, recv_sem, to, source):
@@ -283,13 +286,13 @@
     for copy in push_weight:
         copy.start()
 
-    for copy in copies[1:17]:
+    for copy in copies[1:15]:
         copy.wait()
-    squash = jnp.tanh(matmul(own, decay_first[...])).astype(BF16)
+    squash = jnp.tanh(matmul_t(own, decay_first[...])).astype(BF16)
     pre_decay = vectors[0] + matmul(squash, decay_second[...])
     softplus = jnp.maximum(-pre_decay, 0.0) + jnp.log(1.0 + jnp.exp(-jnp.abs(pre_decay)))
     decay_rate = jnp.exp(-jnp.exp(-softplus - 0.5))
-    low = matmul(own, learn_first[...]).astype(BF16)
+    low = matmul_t(own, learn_first[...]).astype(BF16)
     learn_rate = sigmoid(vectors[1] + matmul(low, learn_second[...]))
     key_factor = 1.0 + (learn_rate - 1.0) * vectors[2]
     opened = sigmoid(matmul(own, gate_first[...])).astype(BF16)
@@ -352,21 +355,22 @@
         mixed_rows[rows + t : rows + t + 1, :] = jnp.sum(
             jnp.where(in_head, own_term * value_t, 0.0), 0, keepdims=True
         )
-        columns = jnp.concatenate(
+        columns[t] = jnp.concatenate(
             [jnp.where(in_head, value_t, 0.0), jnp.where(in_head, -removed, 0.0)], 0
         ).astype(BF16)
-        rank_rows = jnp.concatenate([written_t, change_t], 0).astype(BF16)
-        added = lax.dot_general(
-            columns, rank_rows, (((0,), (0,)), ((), ())), preferred_element_type=F32
-        ).reshape(head_count, head_size, head_size)
-        for h in range(head_count):
-            state[t, h] = before[h] * decay_t[h : h + 1, :] + added[h]
-        pltpu.make_async_copy(state.at[t], next_hbm.at[t], state_out_sem.at[t]).start()
+        rank_rows[t] = jnp.concatenate([written_t, change_t], 0).astype(BF16)
 
     normed = mixed_rows[:rows] * vectors[3] + vectors[4]
     mixer_result = ((normed + mixed_rows[rows:]) * gating).astype(BF16).astype(F32)
     mixer_go, mixer_wait, mixer_drain = spread(1, mixer_result)
     mixer_go()
+    for t in range(rows):
+        decay_t = heads[0, pl.ds(t, head_count, stride=rows), :]
+        added = lax.dot_general(
+            columns[t], rank_rows[t], (((0,), (0,)), ((), ())), preferred_element_type=F32
+        ).reshape(head_count, head_size, head_size)
+        for h in range(head_count):
+            next_state[t, h] = state[t, h] * decay_t[h : h + 1, :] + added[h]
     mixer_wait()
     out_go, out_wait, out_drain = partial_product(3, gathered(1))
     out_go()
@@ -396,14 +400,13 @@
 
     held, _ = routing((slots, 1), 0)
     _, shares = routing((1, slots), 1)
-    share = jnp.concatenate(shares, 0)
-    share_high = share.astype(BF16)
-    share_low = (share - share_high.astype(F32)).astype(BF16)
+    share_out[...] = jnp.concatenate(shares, 0)
 
     out_wait()
     hidden = (
         layer_norm(own_wide + summed(3), vectors[5], vectors[6]).astype(BF16).astype(F32)
     )
+    hidden_out[...] = hidden
     outgoing = held[0] * hidden[0:1]
     for t in range(1, rows):
         outgoing = outgoing + held[t] * hidden[t : t + 1]
@@ -414,7 +417,7 @@
         slot_send, slot_recv, slot_send_sem, slot_recv_sem
     )
     slot_go()
-    for copy in copies[17:]:
+    for copy in copies[15:]:
         copy.wait()
     slot_wait()
     arrived = jnp.concatenate([slot_recv[s].astype(F32) for s in range(n)], 0).astype(BF16)
@@ -437,13 +440,37 @@
     slot_drain()
     for copy in push_weight:
         copy.wait_send()
-    for t in range(rows):
-        pltpu.make_async_copy(state.at[t], next_hbm.at[t], state_out_sem.at[t]).wait()
     back_wait()
-    returned = jnp.concatenate([back_recv[e].astype(F32) for e in range(n)], 0).astype(BF16)
-    combined = matmul(share_high, returned) + matmul(share_low, returned)
-    result[...] = layer_norm(hidden + combined, vectors[7], vectors[8]).astype(BF16)
+    returned[...] = back_recv[...]
     back_drain()
+
+
+def finish_kernel(
+    state, returned, hidden, share, gain_hbm, bias_hbm, result_hbm, next_hbm, norm, result, sems
+):
+    rows = state.shape[0]
+    copies = [
+        pltpu.make_async_copy(gain_hbm, norm.at[0], sems.at[0]),
+        pltpu.make_async_copy(bias_hbm, norm.at[1], sems.at[1]),
+    ] + [
+        pltpu.make_async_copy(state.at[t], next_hbm.at[t], sems.at[2 + t]) for t in range(rows)
+    ]
+    for copy in copies:
+        copy.start()
+    share_high = share[...].astype(BF16)
+    share_low = (share[...] - share_high.astype(F32)).astype(BF16)
+    rows_back = jnp.concatenate(
+        [returned[e].astype(F32) for e in range(returned.shape[0])], 0
+    ).astype(BF16)
+    combined = matmul(share_high, rows_back) + matmul(share_low, rows_back)
+    for copy in copies[:2]:
+        copy.wait()
+    result[...] = layer_norm(hidden[...] + combined, norm[0], norm[1]).astype(BF16)
+    last = pltpu.make_async_copy(result, result_hbm, sems.at[2 + rows])
+    last.start()
+    for copy in copies[2:]:
+        copy.wait()
+    last.wait()
 
 
 def body(
@@ -495,7 +522,8 @@
             expert_norm_bias,
         )
     ]
-    anywhere = pl.BlockSpec(memory_space=pl.ANY)
+    decay_first, learn_first = decay_lowrank_first.T, correction_lowrank_first.T
+    anywhere = pl.BlockSpec(memory_space=pltpu.HBM)
     scalars = pl.BlockSpec(memory_space=pltpu.SMEM)
     dma = pltpu.SemaphoreType.DMA
     vmem = pltpu.VMEM
@@ -506,38 +534,39 @@
         value_matrix,
         receptance_matrix,
         mixer_output_weight,
-        decay_lowrank_first,
+        decay_first,
         decay_lowrank_second,
-        correction_lowrank_first,
+        learn_first,
         correction_lowrank_second,
         gate_lowrank_first,
         gate_lowrank_second,
-        *vectors,
+        *vectors[:7],
         self_token_scale,
         expert_gate_weight,
         expert_up_weight,
         expert_down_weight,
     ]
-    return tuple(
-        pl.pallas_call(
+    passed = pl.pallas_call(
             functools.partial(kernel, n, capacity),
             out_shape=(
-                jax.ShapeDtypeStruct(tokens.shape, BF16),
-                jax.ShapeDtypeStruct(prior_state.shape, F32),
+                pltpu.VMEM(prior_state.shape, F32),
+                pltpu.VMEM((n, capacity, width), BF16),
+                pltpu.VMEM(tokens.shape, F32),
+                pltpu.VMEM((rows, n * capacity), F32),
             ),
             in_specs=[scalars, scalars] + [anywhere] * len(operands),
-            out_specs=(pl.BlockSpec(memory_space=pltpu.VMEM), anywhere),
+            out_specs=(pl.BlockSpec(memory_space=pltpu.VMEM),) * 4,
             scratch_shapes=[
                 vmem(tokens.shape, BF16),
                 vmem(prior_state.shape, F32),
                 vmem((4, block, width), BF16),
-                vmem(decay_lowrank_first.shape, BF16),
+                vmem(decay_first.shape, BF16),
                 vmem(decay_lowrank_second.shape, BF16),
-                vmem(correction_lowrank_first.shape, BF16),
+                vmem(learn_first.shape, BF16),
                 vmem(correction_lowrank_second.shape, BF16),
                 vmem(gate_lowrank_first.shape, BF16),
                 vmem(gate_lowrank_second.shape, BF16),
-                vmem((len(vectors), 1, width), F32),
+                vmem((7, 1, width), F32),
                 vmem(self_token_scale.shape, F32),
                 vmem(expert_gate_weight.shape[1:], BF16),
                 vmem(expert_up_weight.shape[1:], BF16),
@@ -549,12 +578,13 @@
                 vmem((n, capacity, width), BF16),
                 vmem((n, capacity, width), BF16),
                 vmem((n, capacity, width), BF16),
-                vmem((n, capacity, width), BF16),
                 vmem((5, head_count * rows, head_size), F32),
                 vmem((rows, width), F32),
                 vmem((2 * rows, width), F32),
-                dma((20,)),
-                dma((rows,)),
+                vmem((rows, 2 * head_count, width), BF16),
+                vmem((rows, 2 * head_count, head_size), BF16),
+                vmem((n, capacity, width), BF16),
+                dma((18,)),
                 dma((rows,)),
                 dma((4,)),
                 dma((4,)),
@@ -569,9 +599,26 @@
                 dma((n,)),
             ],
             compiler_params=pltpu.CompilerParams(
-                collective_id=0, has_side_effects=True, vmem_limit_bytes=60 * 1024 * 1024
+                collective_id=0, has_side_effects=True, vmem_limit_bytes=52 * 1024 * 1024
             ),
         )(routes, routing_weight, *operands)
+    inside = pl.BlockSpec(memory_space=pltpu.VMEM)
+    return tuple(
+        pl.pallas_call(
+            finish_kernel,
+            out_shape=(
+                jax.ShapeDtypeStruct(tokens.shape, BF16),
+                jax.ShapeDtypeStruct(prior_state.shape, F32),
+            ),
+            in_specs=[inside] * 4 + [anywhere] * 2,
+            out_specs=(anywhere, anywhere),
+            scratch_shapes=[
+                vmem((2, 1, width), F32),
+                vmem(tokens.shape, BF16),
+                dma((rows + 3,)),
+            ],
+            compiler_params=pltpu.CompilerParams(vmem_limit_bytes=16 * 1024 * 1024),
+        )(*passed, *vectors[7:])
     )
 
 

time: 57.3 us -> 47.4 us (0.83)
  local copies, waits for them, and re-layouts: 10 us -> 0.01 us
    unnamed x4, local copies, waits for them, and re-layouts: 10 us -> 0.01 us
    pallas_call x1 -> x2, Pallas kernels: 46.2 us -> 46.4 us  [the longest x1 44.3 us: body(): pl.pallas_call(functools.partial(kernel, n, capacity), out_shape=(pltpu.V...]
where the time goes in v2:
time: 47.4 us; the launch traced here: 47.1 us
  Pallas kernels  46.4 us (98%)
  between operations  0.68 us (1%)
    pallas_call x1, Pallas kernels, body(): pl.pallas_call(functools.partial(kernel, n, capacity), out_shape=(pltpu.V...  44.3 us
    pallas_call x1, Pallas kernels, body(): pl.pallas_call(finish_kernel, out_shape=(jax.ShapeDtypeStruct(tokens.shap...  2.09 us

profile of v2, /device:TPU:0, one launch (start us, length us, event | category | flops | bytes accessed | tf_op | source)
XLA Modules:
  0.0 47.1 jit_solution(2157568287898765902)
XLA Ops:
  0.6 0.0 copy-start
  0.6 0.0 copy-start.1
  0.7 44.3 %shard_map.266 = (f32[4,32,64,64]{3,2,1,0:T(8,128)S(1)}, bf16[16,2,2048]{2,1,0:T(2,128)(2,1)S(1)}, f32[4,2048]{1,0:T(4,128)S(1)}, f32[4,32]{1,0:T(4,128)S(1)}) custom-call(s32[4,4]{1,0:T(4,128)} %routes.1, f32[4,4]{1,0:T(4,128)} %routing_weight.1, bf16[4,2048]{1,0:T(4,128)(2,1)} %tokens_hbm.1, f32[4,32,64,64]{3,2,1,0:T(8,128)} %state_hbm.1, ...), custom_call_target="tpu_custom_call" | custom-call | tf_op jit(solution)/shard_map/pallas_call | solution.py:549
  45.0 0.0 copy-done
  45.0 0.0 copy-done.1
  45.0 2.1 %shard_map.267 = (bf16[4,2048]{1,0:T(4,128)(2,1)}, f32[4,32,64,64]{3,2,1,0:T(8,128)}) custom-call(f32[4,32,64,64]{3,2,1,0:T(8,128)S(1)} %get-tuple-element.6.state, bf16[16,2,2048]{2,1,0:T(2,128)(2,1)S(1)} %get-tuple-element.7.returned, f32[4,2048]{1,0:T(4,128)S(1)} %get-tuple-element.8.hidden, f32[4,32]{1,0:T(4,128)S(1)} %get-tuple-element.9.share, ...), custom_call_target="tpu_custom_call" | custom-call | tf_op jit(solution)/shard_map/pallas_call | solution.py:607
Async XLA Ops:
  0.6 44.4 %copy-start = (f32[2048]{0:T(1024)S(1)}, f32[2048]{0:T(1024)}, u32[]{:S(2)}) copy-start(f32[2048]{0:T(1024)} %param.47) | copy-start | bytes 24580
  0.6 44.4 %copy-start.1 = (f32[2048]{0:T(1024)S(1)}, f32[2048]{0:T(1024)}, u32[]{:S(2)}) copy-start(f32[2048]{0:T(1024)} %param.48) | copy-start | bytes 24580

commit v3 on v2

--- a/solution.py
+++ b/solution.py
@@ -219,7 +219,9 @@
 
     def exchange(make, count, own):
         def send(step, carry):
-            make(lax.rem(own + step, count), own).start()
+            away = (step + 1) // 2
+            offset = count // 2 + away * (2 * lax.rem(step, 2) - 1)
+            make(lax.rem(own + offset, count), own).start()
             return carry
 
         def finish(step, carry):
@@ -232,7 +234,7 @@
             return carry
 
         return (
-            lambda: lax.fori_loop(1, count, send, 0),
+            lambda: lax.fori_loop(0, count - 1, send, 0),
             lambda: lax.fori_loop(1, count, finish, 0),
             lambda: lax.fori_loop(1, count, drain, 0),
         )
@@ -283,7 +285,7 @@
     token_go, token_wait, token_drain = spread(0, own_wide)
     pl.semaphore_wait(barrier, n - 1)
     token_go()
-    for copy in push_weight:
+    for copy in push_weight[:3]:
         copy.start()
 
     for copy in copies[1:15]:
@@ -313,6 +315,7 @@
         part = partial_product(i, segment)
         part[0]()
         parts.append(part)
+    push_weight[3].start()
     parts[0][1]()
     by_head(3, summed(0))
     parts[1][1]()

time: 47.4 us -> 49.7 us (1.049)
  Pallas kernels: 46.4 us -> 48.8 us
    pallas_call x1, Pallas kernels: 44.3 us -> 46.7 us  [body(): pl.pallas_call(functools.partial(kernel, n, capacity), out_shape=(pltpu.V...]
where the time goes in v3:
time: 49.7 us; the launch traced here: 49.5 us
  Pallas kernels  48.8 us (98%)
  between operations  0.68 us (1%)
    pallas_call x1, Pallas kernels, body(): pl.pallas_call(functools.partial(kernel, n, capacity), out_shape=(pltpu.V...  46.7 us
    pallas_call x1, Pallas kernels, body(): pl.pallas_call(finish_kernel, out_shape=(jax.ShapeDtypeStruct(tokens.shap...  2.09 us

profile of v3, /device:TPU:0, one launch (start us, length us, event | category | flops | bytes accessed | tf_op | source)
XLA Modules:
  0.0 49.5 jit_solution(554881946433918979)
XLA Ops:
  0.6 0.0 copy-start
  0.6 0.0 copy-start.1
  0.7 46.7 %shard_map.266 = (f32[4,32,64,64]{3,2,1,0:T(8,128)S(1)}, bf16[16,2,2048]{2,1,0:T(2,128)(2,1)S(1)}, f32[4,2048]{1,0:T(4,128)S(1)}, f32[4,32]{1,0:T(4,128)S(1)}) custom-call(s32[4,4]{1,0:T(4,128)} %routes.1, f32[4,4]{1,0:T(4,128)} %routing_weight.1, bf16[4,2048]{1,0:T(4,128)(2,1)} %tokens_hbm.1, f32[4,32,64,64]{3,2,1,0:T(8,128)} %state_hbm.1, ...), custom_call_target="tpu_custom_call" | custom-call | tf_op jit(solution)/shard_map/pallas_call | solution.py:552
  47.4 0.0 copy-done
  47.4 0.0 copy-done.1
  47.4 2.1 %shard_map.267 = (bf16[4,2048]{1,0:T(4,128)(2,1)}, f32[4,32,64,64]{3,2,1,0:T(8,128)}) custom-call(f32[4,32,64,64]{3,2,1,0:T(8,128)S(1)} %get-tuple-element.6.state, bf16[16,2,2048]{2,1,0:T(2,128)(2,1)S(1)} %get-tuple-element.7.returned, f32[4,2048]{1,0:T(4,128)S(1)} %get-tuple-element.8.hidden, f32[4,32]{1,0:T(4,128)S(1)} %get-tuple-element.9.share, ...), custom_call_target="tpu_custom_call" | custom-call | tf_op jit(solution)/shard_map/pallas_call | solution.py:610
Async XLA Ops:
  0.6 46.7 %copy-start = (f32[2048]{0:T(1024)S(1)}, f32[2048]{0:T(1024)}, u32[]{:S(2)}) copy-start(f32[2048]{0:T(1024)} %param.47) | copy-start | bytes 24580
  0.6 46.7 %copy-start.1 = (f32[2048]{0:T(1024)S(1)}, f32[2048]{0:T(1024)}, u32[]{:S(2)}) copy-start(f32[2048]{0:T(1024)} %param.48) | copy-start | bytes 24580
